TPU v7x, 32 devices: a whole 2x2x4 slice. The times are simulated.
32 devices in a mesh: grp: 2 (over x), sp: 4 (over z), tp: 4 (over y, core).
Axes of the slice: x: 2, y: 2, z: 4, core: 2. Of those that a mesh axis runs over, the one named last changes fastest.
Arguments:
- tokens: bfloat16 [1792, 4096], P(('grp', 'sp'), 'tp'), parts along dimension 0, may hold values from -130 to 130
- rms_gain: float32 [2, 4096], replicated, may hold values from 0.1 to 1.9
- w_value: bfloat16 [2, 4096, 2048], P(None, 'sp', 'tp'), may hold values from -0.09375 to 0.09375
- w_gate: bfloat16 [2, 4096, 2048], P(None, 'sp', 'tp'), may hold values from -0.09375 to 0.09375
- taps: float32 [2, 31, 2048], P(None, None, 'tp'), may hold values from -8 to 8
- ln_gain: float32 [2, 2048], P(None, 'tp'), may hold values from 0.1 to 1.9
- ln_bias: float32 [2, 2048], P(None, 'tp'), may hold values from -3 to 3
- w_out: bfloat16 [2, 2048, 4096], P(None, 'sp', 'tp'), may hold values from -0.125 to 0.125
Outputs:
- result: bfloat16 [1792, 4096], P(('grp', 'sp'), 'tp'), parts along dimension 0
There are 2 independent parts, one for each index of `grp`. A program takes and returns all parts, laid end to end along the dimension named above; an argument that names none is the same for every part. Nothing has to cross between parts.
All inputs are finite; a program needn't handle non-finite values.
Results may differ from a plain program's by a relative error of at most 0.009.
Values may be sent and summed in bfloat16 or wider, within the bound.
A program may use at most 64 MiB of HBM per device.

v0:
```python
import jax
import jax.numpy as jnp
from jax import lax
from jax.sharding import PartitionSpec as P

CH = 2048


def passed_along(block, axis, distance):
    devices = range(lax.axis_size(axis))
    route = [(i - distance, i) for i in devices if i - distance in devices]
    return lax.ppermute(block, axis, route)


def project_in(weight, columns):
    return lax.dot_general(
        weight, columns, (((0,), (1,)), ((), ())), preferred_element_type=jnp.float32
    )


def project_out(rows, weight):
    return lax.dot_general(
        rows, weight, (((0,), (0,)), ((), ())), preferred_element_type=jnp.float32
    )


def norm_rows(wide, gain):
    return (wide * lax.rsqrt(jnp.mean(wide * wide, axis=1, keepdims=True) + 1e-06) * gain).astype(
        jnp.bfloat16
    )


def shards(tokens, rms_gain, w_value, w_gate, taps, ln_gain, ln_bias, w_out):
    layers = w_value.shape[0]
    tok_rows = tokens.shape[0]
    chans = w_value.shape[2]
    reach = taps.shape[1]
    current = tokens
    for layer in range(layers):
        gain = rms_gain[layer]
        whole_rows = lax.all_gather(current, "tp", axis=1, tiled=True)
        normed = norm_rows(whole_rows.astype(jnp.float32), gain)
        value_t = project_in(lax.all_gather(w_value[layer], "sp", axis=0, tiled=True), normed)
        gate_t = project_in(lax.all_gather(w_gate[layer], "sp", axis=0, tiled=True), normed)
        glu_t = (value_t * jax.nn.sigmoid(gate_t)).astype(jnp.bfloat16)
        earlier = passed_along(glu_t[:, tok_rows - (reach - 1) :], "sp", 1)
        extended = jnp.concatenate([earlier, glu_t], axis=1).astype(jnp.float32)
        layer_taps = taps[layer]
        conv = jnp.zeros((chans, tok_rows), jnp.float32)
        for k in range(reach):
            conv = conv + layer_taps[k][:, None] * extended[:, k : k + tok_rows]
        total, total_sq = lax.psum((jnp.sum(conv, axis=0), jnp.sum(conv * conv, axis=0)), "tp")
        mean = total / CH
        var = total_sq / CH - mean * mean
        shaped = (conv - mean[None, :]) * lax.rsqrt(var + 1e-05)[None, :] * ln_gain[layer][
            :, None
        ] + ln_bias[layer][:, None]
        act_t = jax.nn.silu(shaped).astype(jnp.bfloat16)
        act_all = lax.all_gather(act_t, "tp", axis=0, tiled=True)
        branch = project_out(act_all, lax.all_gather(w_out[layer], "sp", axis=0, tiled=True))
        current = (current.astype(jnp.float32) + branch).astype(jnp.bfloat16)
    return current


def solution(mesh):
    return jax.shard_map(
        shards,
        mesh=mesh,
        in_specs=(
            P(("grp", "sp"), "tp"),
            P(),
            P(None, "sp", "tp"),
            P(None, "sp", "tp"),
            P(None, None, "tp"),
            P(None, "tp"),
            P(None, "tp"),
            P(None, "sp", "tp"),
        ),
        out_specs=P(("grp", "sp"), "tp"),
        check_vma=False,
    )
```

profile of v0, /device:TPU:0, one launch (start us, length us, event | category | flops | bytes accessed | tf_op | source)
XLA Modules:
  0.0 555.3 jit_solution(11916564640636365866)
XLA Ops:
  6.5 0.7 all-gather.15.cloned.1.call-update
  7.3 0.0 all-gather.21.cloned.1.call-start
  7.3 3.0 fusion.142
  10.3 0.0 all-gather.21.cloned.1.call-update
  10.3 0.0 all-gather.19.cloned.1.call-start
  10.4 1.5 fusion.141
  11.9 0.0 all-gather.19.cloned.1.call-update
  11.9 0.0 all-gather.23.cloned.1.call-start
  11.9 3.0 fusion.140
  15.0 0.0 all-gather.23.cloned.1.call-update
  15.0 0.0 all-gather.17.cloned.1.call-start
  15.2 17.5 %all-gather.15.cloned.1.call-done = bf16[224,4096]{1,0:T(8,128)(2,1)} async-done(((bf16[224,1024]{1,0:T(8,128)(2,1)}), bf16[224,4096]{1,0:T(8,128)(2,1)}) %all-gather.15.cloned.1.call-update) | async-done | bytes 1835024 | tf_op jit(solution)/shard_map/all_gather | solution.py:41
  32.8 1.9 fusion.12
  34.7 80.4 %all-gather.21.cloned.1.call-done = bf16[1,4096,512]{2,1,0:T(8,128)(2,1)} async-done(((bf16[1,1024,512]{2,1,0:T(8,128)(2,1)}), bf16[1,4096,512]{2,1,0:T(8,128)(2,1)}) %all-gather.21.cloned.1.call-update) | async-done | bytes 4194320 | tf_op jit(solution)/shard_map/all_gather | solution.py:44
  115.1 4.1 fusion.57
  119.2 76.7 %all-gather.19.cloned.1.call-done = bf16[1,4096,512]{2,1,0:T(8,128)(2,1)} async-done(((bf16[1,1024,512]{2,1,0:T(8,128)(2,1)}), bf16[1,4096,512]{2,1,0:T(8,128)(2,1)}) %all-gather.19.cloned.1.call-update) | async-done | bytes 4194320 | tf_op jit(solution)/shard_map/all_gather | solution.py:43
  195.9 3.3 fusion.66
  199.3 1.3 collective-permute-start
  200.6 1.6 collective-permute-done
  202.2 0.1 maximum_convert_fusion
  202.2 2.4 fusion.137
  204.6 6.3 %all-reduce.1 = (f32[224]{0:T(256)S(1)}, f32[224]{0:T(256)S(1)}) all-reduce(f32[224]{0:T(256)S(1)} %get-tuple-element.8, f32[224]{0:T(256)S(1)} %get-tuple-element.7), channel_id=1, replica_groups=mesh['grp'=2,'sp'=4,'tp'=4] {'tp'}, use_global_device_ids=true, to_apply=%region_4.0 | all-reduce | flops 448 | bytes 3584 | tf_op jit(solution)/shard_map/psum | solution.py:52
  210.9 0.2 multiply_convert_fusion.1
  211.2 9.1 %all_gather.33 = bf16[2048,224]{0,1:T(8,128)(2,1)S(1)} all-gather(bf16[512,224]{0,1:T(8,128)(2,1)S(1)} %multiply_convert_fusion.1), channel_id=1, replica_groups=mesh['grp'=2,'sp'=4,'tp'=4] {'tp'}, dimensions={0}, use_global_device_ids=true | all-gather | bytes 1146880 | tf_op jit(solution)/shard_map/all_gather | solution.py:59
  220.3 56.3 %all-gather.23.cloned.1.call-done = bf16[1,2048,1024]{2,1,0:T(8,128)(2,1)} async-done(((bf16[1,512,1024]{2,1,0:T(8,128)(2,1)}), bf16[1,2048,1024]{2,1,0:T(8,128)(2,1)}) %all-gather.23.cloned.1.call-update) | async-done | bytes 4194320 | tf_op jit(solution)/shard_map/all_gather | solution.py:60
  276.6 4.1 fusion.27
  280.7 0.0 all-gather.17.cloned.1.call-update
  280.7 0.0 all-gather.27.cloned.1.call-start
  280.8 0.5 all-gather.27.cloned.1.call-update
  281.3 0.0 all-gather.25.cloned.1.call-start
  281.4 0.7 all-gather.25.cloned.1.call-update
  282.1 0.0 all-gather.29.cloned.1.call-start
  282.1 0.7 all-gather.29.cloned.1.call-update
  282.8 17.7 %all-gather.17.cloned.1.call-done = bf16[224,4096]{1,0:T(8,128)(2,1)} async-done(((bf16[224,1024]{1,0:T(8,128)(2,1)}), bf16[224,4096]{1,0:T(8,128)(2,1)}) %all-gather.17.cloned.1.call-update) | async-done | bytes 1835024 | tf_op jit(solution)/shard_map/all_gather | solution.py:41
  300.5 1.9 fusion.15
  302.4 80.2 %all-gather.27.cloned.1.call-done = bf16[1,4096,512]{2,1,0:T(8,128)(2,1)} async-done(((bf16[1,1024,512]{2,1,0:T(8,128)(2,1)}), bf16[1,4096,512]{2,1,0:T(8,128)(2,1)}) %all-gather.27.cloned.1.call-update) | async-done | bytes 4194320 | tf_op jit(solution)/shard_map/all_gather | solution.py:44
  382.7 4.1 fusion.51
  386.8 76.7 %all-gather.25.cloned.1.call-done = bf16[1,4096,512]{2,1,0:T(8,128)(2,1)} async-done(((bf16[1,1024,512]{2,1,0:T(8,128)(2,1)}), bf16[1,4096,512]{2,1,0:T(8,128)(2,1)}) %all-gather.25.cloned.1.call-update) | async-done | bytes 4194320 | tf_op jit(solution)/shard_map/all_gather | solution.py:43
  463.5 3.3 fusion.69
  466.9 1.3 collective-permute-start.1
  468.2 1.5 collective-permute-done.1
  469.7 0.1 maximum_convert_fusion.1
  469.8 2.4 fusion.136
  472.2 6.3 %all-reduce = (f32[224]{0:T(256)S(1)}, f32[224]{0:T(256)S(1)}) all-reduce(f32[224]{0:T(256)S(1)} %get-tuple-element.6, f32[224]{0:T(256)S(1)} %get-tuple-element.5), channel_id=1, replica_groups=mesh['grp'=2,'sp'=4,'tp'=4] {'tp'}, use_global_device_ids=true, to_apply=%region_9.10 | all-reduce | flops 448 | bytes 3584 | tf_op jit(solution)/shard_map/psum | solution.py:52
  478.5 0.2 multiply_convert_fusion
  478.8 9.1 %all_gather.38 = bf16[2048,224]{0,1:T(8,128)(2,1)S(1)} all-gather(bf16[512,224]{0,1:T(8,128)(2,1)S(1)} %multiply_convert_fusion), channel_id=1, replica_groups=mesh['grp'=2,'sp'=4,'tp'=4] {'tp'}, dimensions={0}, use_global_device_ids=true | all-gather | bytes 1146880 | tf_op jit(solution)/shard_map/all_gather | solution.py:59
  487.9 56.5 %all-gather.29.cloned.1.call-done = bf16[1,2048,1024]{2,1,0:T(8,128)(2,1)} async-done(((bf16[1,512,1024]{2,1,0:T(8,128)(2,1)}), bf16[1,2048,1024]{2,1,0:T(8,128)(2,1)}) %all-gather.29.cloned.1.call-update) | async-done | bytes 4194320 | tf_op jit(solution)/shard_map/all_gather | solution.py:60
  544.3 4.1 fusion.24
  (32 shorter events, 0.3 us)
Async XLA Ops:
  6.5 3.9 copy-start
  6.5 26.2 %all-gather.15.cloned.1.call-start = ((), (), s32[]{:S(2)}) async-start(), calls=%async_computation | async-start | bytes 2293760 | tf_op jit(solution)/shard_map/all_gather | solution.py:41
  7.3 107.8 %all-gather.21.cloned.1.call-start = ((), (), s32[]{:S(2)}) async-start(), calls=%async_computation.3 | async-start | bytes 5242880 | tf_op jit(solution)/shard_map/all_gather | solution.py:44
  10.3 185.6 %all-gather.19.cloned.1.call-start = ((), (), s32[]{:S(2)}) async-start(), calls=%async_computation.2 | async-start | bytes 5242880 | tf_op jit(solution)/shard_map/all_gather | solution.py:43
  11.9 3.2 copy-start.7
  11.9 3.2 copy-start.5
  11.9 3.3 copy-start.6
  11.9 264.7 %all-gather.23.cloned.1.call-start = ((), (), s32[]{:S(2)}) async-start(), calls=%async_computation.4 | async-start | bytes 5242880 | tf_op jit(solution)/shard_map/all_gather | solution.py:60
  15.0 285.5 %all-gather.17.cloned.1.call-start = ((), (), s32[]{:S(2)}) async-start(), calls=%async_computation.1 | async-start | bytes 2293760 | tf_op jit(solution)/shard_map/all_gather | solution.py:41
  115.1 80.8 %copy-start.1 = (bf16[224,4096]{1,0:T(8,128)(2,1)S(1)}, bf16[224,4096]{1,0:T(8,128)(2,1)}, u32[]{:S(2)}) copy-start(bf16[224,4096]{1,0:T(8,128)(2,1)} %all-gather.15.cloned.1.call-done) | copy-start | bytes 5505028
  119.2 81.4 %copy-start.8 = (f32[2,512]{1,0:T(2,128)S(1)}, f32[2,512]{1,0:T(2,128)}, u32[]{:S(2)}) copy-start(f32[2,512]{1,0:T(2,128)} %param.14) | copy-start | bytes 12292
  199.3 2.9 collective-permute-start
  202.2 74.4 %copy-start.3 = (bf16[224,1024]{1,0:T(8,128)(2,1)S(1)}, bf16[224,1024]{1,0:T(8,128)(2,1)}, u32[]{:S(2)}) copy-start(bf16[224,1024]{1,0:T(8,128)(2,1)} %param.8) | copy-start | bytes 1376260
  280.7 101.9 %all-gather.27.cloned.1.call-start = ((), (), s32[]{:S(2)}) async-start(), calls=%async_computation.6 | async-start | bytes 5242880 | tf_op jit(solution)/shard_map/all_gather | solution.py:44
  281.3 182.2 %all-gather.25.cloned.1.call-start = ((), (), s32[]{:S(2)}) async-start(), calls=%async_computation.5 | async-start | bytes 5242880 | tf_op jit(solution)/shard_map/all_gather | solution.py:43
  282.1 262.3 %all-gather.29.cloned.1.call-start = ((), (), s32[]{:S(2)}) async-start(), calls=%async_computation.7 | async-start | bytes 5242880 | tf_op jit(solution)/shard_map/all_gather | solution.py:60
  382.7 80.8 %copy-start.2 = (bf16[224,4096]{1,0:T(8,128)(2,1)S(1)}, bf16[224,4096]{1,0:T(8,128)(2,1)}, u32[]{:S(2)}) copy-start(bf16[224,4096]{1,0:T(8,128)(2,1)} %all-gather.17.cloned.1.call-done) | copy-start | bytes 5505028
  466.9 2.9 collective-permute-start.1
  469.8 74.5 %copy-start.4 = (bf16[224,1024]{1,0:T(8,128)(2,1)S(1)}, bf16[224,1024]{1,0:T(8,128)(2,1)}, u32[]{:S(2)}) copy-start(bf16[224,1024]{1,0:T(8,128)(2,1)} %fusion.27) | copy-start | bytes 1376260
Sparse Core Ops, SparseCore 0:
  8.9 23.8 all-gather.14
  34.3 80.7 all-gather.20
  116.7 79.2 all-gather.18
  197.3 79.2 all-gather.22
  280.8 19.5 all-gather.16
  301.9 80.7 all-gather.26
  384.2 79.2 all-gather.24
  465.1 79.2 all-gather.28
where the time goes:
time: 556 us; the launch traced here: 555 us
  waiting for transfers between devices  468 us (84%)
  blocking collectives  30.7 us (6%)
  matrix products  23.1 us (4%)
  between operations  13.7 us (2%)
  other arithmetic  9.31 us (2%)
  local copies, waits for them, and re-layouts  7.75 us (1%)
    all_gather x2, waiting for transfers between devices, shards(): lax.all_gather(w_gate[layer], 'sp', axis=0, tiled=True)  161 us
    all_gather x2, waiting for transfers between devices, shards(): lax.all_gather(w_value[layer], 'sp', axis=0, tiled=True)  153 us
    all_gather x2, waiting for transfers between devices, shards(): lax.all_gather(w_out[layer], 'sp', axis=0, tiled=True)  113 us
    all_gather x2, waiting for transfers between devices, shards(): whole_rows = lax.all_gather(current, 'tp', axis=1, tiled=True)  35.2 us
    all_gather x2, blocking collectives, shards(): act_all = lax.all_gather(act_t, 'tp', axis=0, tiled=True)  18.2 us
    dot_general x4, matrix products, project_in(): lax.dot_general(weight, columns, (((0,), (1,)), ((), ())), preferred_elem...  14.9 us
    psum x2, blocking collectives, shards(): lax.psum((jnp.sum(conv, axis=0), jnp.sum(conv * conv, axis=0)), 'tp')  12.5 us
  transfers between devices with their start and end apart: 10, of which 10 were waited for; matrix products, arithmetic and copies ran while one was open for 6% of the time, Pallas kernels for 0%

commit v1 on v0

--- a/solution.py
+++ b/solution.py
@@ -38,7 +38,9 @@
     current = tokens
     for layer in range(layers):
         gain = rms_gain[layer]
-        whole_rows = lax.all_gather(current, "tp", axis=1, tiled=True)
+        whole_rows = jnp.concatenate(
+            lax.all_to_all(jnp.stack([current] * lax.axis_size("tp")), "tp", 0, 0), axis=1
+        )
         normed = norm_rows(whole_rows.astype(jnp.float32), gain)
         value_t = project_in(lax.all_gather(w_value[layer], "sp", axis=0, tiled=True), normed)
         gate_t = project_in(lax.all_gather(w_gate[layer], "sp", axis=0, tiled=True), normed)

time: 556 us -> 508 us (0.914)
  waiting for transfers between devices: 468 us -> 384 us
  blocking collectives: 30.7 us -> 56.1 us
  local copies, waits for them, and re-layouts: 7.75 us -> 14.2 us
    all_gather x2, waiting for transfers between devices: 161 us -> 94.5 us  [shards(): lax.all_gather(w_gate[layer], 'sp', axis=0, tiled=True)]
    all_gather x2 -> x0, waiting for transfers between devices: 35.2 us -> none  [shards(): whole_rows = lax.all_gather(current, 'tp', axis=1, tiled=True)]
    all_to_all x0 -> x1, blocking collectives: none -> 25.4 us  [shards(): lax.all_to_all(jnp.stack([current] * lax.axis_size('tp')), 'tp', 0, 0)]
    all_to_all x0 -> x1, waiting for transfers between devices: none -> 22.2 us  [shards(): lax.all_to_all(jnp.stack([current] * lax.axis_size('tp')), 'tp', 0, 0)]
  transfers between devices with their start and end apart: 10 -> 9, of which waited for: 10 -> 9; matrix products, arithmetic and copies ran while one was open for 6% -> 8% of each run, Pallas kernels for 0% -> 0%
where the time goes in v1:
time: 508 us
  waiting for transfers between devices  384 us (76%)
  blocking collectives  56.1 us (11%)
  matrix products  25.4 us (5%)
  local copies, waits for them, and re-layouts  14.2 us (3%)
  between operations  13.7 us (3%)
  other arithmetic  7.1 us (1%)
  starting transfers between devices  7.01 us (1%)
    all_gather x2, waiting for transfers between devices, shards(): lax.all_gather(w_value[layer], 'sp', axis=0, tiled=True)  152 us
    all_gather x2, waiting for transfers between devices, shards(): lax.all_gather(w_out[layer], 'sp', axis=0, tiled=True)  111 us
    all_gather x2, waiting for transfers between devices, shards(): lax.all_gather(w_gate[layer], 'sp', axis=0, tiled=True)  94.5 us
    all_to_all x1, blocking collectives, shards(): lax.all_to_all(jnp.stack([current] * lax.axis_size('tp')), 'tp', 0, 0)  25.4 us
    all_to_all x1, waiting for transfers between devices, shards(): lax.all_to_all(jnp.stack([current] * lax.axis_size('tp')), 'tp', 0, 0)  22.2 us
    all_gather x2, blocking collectives, shards(): act_all = lax.all_gather(act_t, 'tp', axis=0, tiled=True)  18.2 us
    dot_general x4, matrix products, project_in(): lax.dot_general(weight, columns, (((0,), (1,)), ((), ())), preferred_elem...  18 us
    psum x2, blocking collectives, shards(): lax.psum((jnp.sum(conv, axis=0), jnp.sum(conv * conv, axis=0)), 'tp')  12.5 us
  transfers between devices with their start and end apart: 9, of which 9 were waited for; matrix products, arithmetic and copies ran while one was open for 8% of the time, Pallas kernels for 0%

profile of v1, /device:TPU:0, one launch (start us, length us, event | category | flops | bytes accessed | tf_op | source)
XLA Modules:
  0.0 508.0 jit_solution(2979847719748121921)
XLA Ops:
  6.5 3.2 fusion.134
  9.7 0.0 all-gather.15.cloned.1.call-update
  9.8 0.0 all-gather.13.cloned.1.call-start
  9.8 1.5 fusion.133
  11.4 0.0 all-gather.17.cloned.1.call-start
  11.4 3.1 fusion.132
  14.6 0.0 all-gather.21.cloned.1.call-start
  14.6 0.5 all-gather.21.cloned.1.call-update
  15.1 0.0 all-gather.19.cloned.1.call-start
  15.2 0.5 all-gather.19.cloned.1.call-update
  15.8 1.5 stack.4
  17.3 4.3 all-to-all-start
  21.5 0.6 all-gather.23.cloned.1.call-update
  22.3 22.2 %all-to-all-done = bf16[4,224,1024]{2,1,0:T(8,128)(2,1)S(1)} async-done(((bf16[4,224,1024]{2,1,0:T(8,128)(2,1)}), bf16[4,224,1024]{2,1,0:T(8,128)(2,1)S(1)}, u32[]{:S(2)}, u32[]{:S(2)}) %all-to-all-start) | async-done | bytes 1835040 | tf_op jit(solution)/shard_map/all_to_all | solution.py:42
  44.4 0.4 convert_bitcast_fusion.1
  44.8 2.2 copy.11
  47.1 0.4 fusion.12
  47.5 45.8 %all-gather.15.cloned.1.call-done = bf16[1,4096,512]{2,1,0:T(8,128)(2,1)} async-done(((bf16[1,1024,512]{2,1,0:T(8,128)(2,1)}), bf16[1,4096,512]{2,1,0:T(8,128)(2,1)}) %all-gather.15.cloned.1.call-update) | async-done | bytes 4194320 | tf_op jit(solution)/shard_map/all_gather | solution.py:46
  93.4 4.5 fusion.53
  97.9 76.3 %all-gather.13.cloned.1.call-done = bf16[1,4096,512]{2,1,0:T(8,128)(2,1)} async-done(((bf16[1,1024,512]{2,1,0:T(8,128)(2,1)}), bf16[1,4096,512]{2,1,0:T(8,128)(2,1)}) %all-gather.13.cloned.1.call-update) | async-done | bytes 4194320 | tf_op jit(solution)/shard_map/all_gather | solution.py:45
  174.2 4.5 fusion.62
  178.7 1.3 collective-permute-start
  180.0 1.6 collective-permute-done
  181.6 0.1 maximum_convert_fusion
  181.6 2.4 fusion.129
  184.0 6.3 %all-reduce.1 = (f32[224]{0:T(256)S(1)}, f32[224]{0:T(256)S(1)}) all-reduce(f32[224]{0:T(256)S(1)} %get-tuple-element.8, f32[224]{0:T(256)S(1)} %get-tuple-element.7), channel_id=1, replica_groups=mesh['grp'=2,'sp'=4,'tp'=4] {'tp'}, use_global_device_ids=true, to_apply=%region_4.0 | all-reduce | flops 448 | bytes 3584 | tf_op jit(solution)/shard_map/psum | solution.py:54
  190.3 0.2 multiply_convert_fusion.3
  190.6 9.1 %all_gather.26 = bf16[2048,224]{0,1:T(8,128)(2,1)S(1)} all-gather(bf16[512,224]{0,1:T(8,128)(2,1)S(1)} %multiply_convert_fusion.3), channel_id=1, replica_groups=mesh['grp'=2,'sp'=4,'tp'=4] {'tp'}, dimensions={0}, use_global_device_ids=true | all-gather | bytes 1146880 | tf_op jit(solution)/shard_map/all_gather | solution.py:61
  199.7 55.4 %all-gather.17.cloned.1.call-done = bf16[1,2048,1024]{2,1,0:T(8,128)(2,1)} async-done(((bf16[1,512,1024]{2,1,0:T(8,128)(2,1)}), bf16[1,2048,1024]{2,1,0:T(8,128)(2,1)}) %all-gather.17.cloned.1.call-update) | async-done | bytes 4194320 | tf_op jit(solution)/shard_map/all_gather | solution.py:62
  255.0 3.3 fusion.23
  258.3 0.2 stack.5
  258.6 25.4 %all_to_all.10 = bf16[4,224,1024]{2,1,0:T(8,128)(2,1)S(1)} all-to-all(bf16[4,224,1024]{2,1,0:T(8,128)(2,1)S(1)} %stack.5), channel_id=1, replica_groups=mesh['grp'=2,'sp'=4,'tp'=4] {'tp'}, dimensions={0} | all-to-all | bytes 3670016 | tf_op jit(solution)/shard_map/all_to_all | solution.py:42
  284.0 0.4 convert_bitcast_fusion
  284.4 2.2 copy.12
  286.6 0.4 fusion.13
  287.1 48.7 %all-gather.21.cloned.1.call-done = bf16[1,4096,512]{2,1,0:T(8,128)(2,1)} async-done(((bf16[1,1024,512]{2,1,0:T(8,128)(2,1)}), bf16[1,4096,512]{2,1,0:T(8,128)(2,1)}) %all-gather.21.cloned.1.call-update) | async-done | bytes 4194320 | tf_op jit(solution)/shard_map/all_gather | solution.py:46
  335.7 4.5 fusion.47
  340.3 76.1 %all-gather.19.cloned.1.call-done = bf16[1,4096,512]{2,1,0:T(8,128)(2,1)} async-done(((bf16[1,1024,512]{2,1,0:T(8,128)(2,1)}), bf16[1,4096,512]{2,1,0:T(8,128)(2,1)}) %all-gather.19.cloned.1.call-update) | async-done | bytes 4194320 | tf_op jit(solution)/shard_map/all_gather | solution.py:45
  416.4 4.5 fusion.65
  420.9 1.3 collective-permute-start.1
  422.2 1.5 collective-permute-done.1
  423.8 0.1 maximum_convert_fusion.1
  423.8 2.4 fusion.128
  426.2 6.3 %all-reduce = (f32[224]{0:T(256)S(1)}, f32[224]{0:T(256)S(1)}) all-reduce(f32[224]{0:T(256)S(1)} %get-tuple-element.6, f32[224]{0:T(256)S(1)} %get-tuple-element.5), channel_id=1, replica_groups=mesh['grp'=2,'sp'=4,'tp'=4] {'tp'}, use_global_device_ids=true, to_apply=%region_9.10 | all-reduce | flops 448 | bytes 3584 | tf_op jit(solution)/shard_map/psum | solution.py:54
  432.5 0.2 multiply_convert_fusion.2
  432.7 9.1 %all_gather.30 = bf16[2048,224]{0,1:T(8,128)(2,1)S(1)} all-gather(bf16[512,224]{0,1:T(8,128)(2,1)S(1)} %multiply_convert_fusion.2), channel_id=1, replica_groups=mesh['grp'=2,'sp'=4,'tp'=4] {'tp'}, dimensions={0}, use_global_device_ids=true | all-gather | bytes 1146880 | tf_op jit(solution)/shard_map/all_gather | solution.py:61
  441.8 55.2 %all-gather.23.cloned.1.call-done = bf16[1,2048,1024]{2,1,0:T(8,128)(2,1)} async-done(((bf16[1,512,1024]{2,1,0:T(8,128)(2,1)}), bf16[1,2048,1024]{2,1,0:T(8,128)(2,1)}) %all-gather.23.cloned.1.call-update) | async-done | bytes 4194320 | tf_op jit(solution)/shard_map/all_gather | solution.py:62
  497.1 4.1 fusion.20
  (29 shorter events, 0.3 us)
Async XLA Ops:
  6.5 3.3 copy-start
  6.5 86.8 %all-gather.15.cloned.1.call-start = ((), (), s32[]{:S(2)}) async-start(), calls=%async_computation.3 | async-start | bytes 5242880 | tf_op jit(solution)/shard_map/all_gather | solution.py:46
  9.8 164.4 %all-gather.13.cloned.1.call-start = ((), (), s32[]{:S(2)}) async-start(), calls=%async_computation.2 | async-start | bytes 5242880 | tf_op jit(solution)/shard_map/all_gather | solution.py:45
  11.3 4.4 copy-start.1
  11.4 243.7 %all-gather.17.cloned.1.call-start = ((), (), s32[]{:S(2)}) async-start(), calls=%async_computation.4 | async-start | bytes 5242880 | tf_op jit(solution)/shard_map/all_gather | solution.py:62
  14.6 321.2 %all-gather.21.cloned.1.call-start = ((), (), s32[]{:S(2)}) async-start(), calls=%async_computation.6 | async-start | bytes 5242880 | tf_op jit(solution)/shard_map/all_gather | solution.py:46
  15.1 401.3 %all-gather.19.cloned.1.call-start = ((), (), s32[]{:S(2)}) async-start(), calls=%async_computation.5 | async-start | bytes 5242880 | tf_op jit(solution)/shard_map/all_gather | solution.py:45
  15.7 6.4 %copy-start.2 = (f32[2,31,512]{2,0,1:T(2,128)S(1)}, f32[2,31,512]{2,0,1:T(2,128)}, u32[]{:S(2)}) copy-start(f32[2,31,512]{2,0,1:T(2,128)} %param.12) | copy-start | bytes 380932
  15.7 6.4 %copy-start.4 = (f32[2,512]{1,0:T(2,128)S(1)}, f32[2,512]{1,0:T(2,128)}, u32[]{:S(2)}) copy-start(f32[2,512]{1,0:T(2,128)} %param.13) | copy-start | bytes 12292
  15.8 6.5 %copy-start.3 = (f32[2,4096]{1,0:T(2,128)S(1)}, f32[2,4096]{1,0:T(2,128)}, u32[]{:S(2)}) copy-start(f32[2,4096]{1,0:T(2,128)} %param.9) | copy-start | bytes 98308
  17.3 27.2 %all-to-all-start = ((bf16[4,224,1024]{2,1,0:T(8,128)(2,1)}), bf16[4,224,1024]{2,1,0:T(8,128)(2,1)S(1)}, u32[]{:S(2)}, u32[]{:S(2)}) async-start(bf16[4,224,1024]{2,1,0:T(8,128)(2,1)} %stack.4), calls=%async_computation | async-start | bytes 3670016 | tf_op jit(solution)/shard_map/all_to_all | solution.py:42
  21.5 475.5 %all-gather.23.cloned.1.call-start = ((), (), s32[]{:S(2)}) async-start(), calls=%async_computation.7 | async-start | bytes 5242880 | tf_op jit(solution)/shard_map/all_gather | solution.py:62
  97.9 82.1 %copy-start.5 = (f32[2,512]{1,0:T(2,128)S(1)}, f32[2,512]{1,0:T(2,128)}, u32[]{:S(2)}) copy-start(f32[2,512]{1,0:T(2,128)} %param.14) | copy-start | bytes 12292
  178.7 2.9 collective-permute-start
  420.9 2.9 collective-permute-start.1
Sparse Core Ops, SparseCore 0:
  9.9 83.4 all-gather.14
  94.9 79.2 all-gather.12
  175.8 79.2 all-gather.16
  256.5 79.2 all-gather.20
  337.1 79.2 all-gather.18
  417.8 79.2 all-gather.22
